TPU v7x, 32 devices: a whole 2x2x4 slice. The times are simulated.
32 devices in a mesh: tp: 8 (over z, y), dp: 4 (over x, core).
Axes of the slice: x: 2, y: 2, z: 4, core: 2. Of those that a mesh axis runs over, the one named last changes fastest.
Arguments:
- stream: bfloat16 [256, 2048], P('tp', 'dp'), may hold values from -12 to 12
- norm_gain: float32 [2, 2048], P(None, 'dp'), may hold values from 0.1 to 1.9
- w_input: bfloat16 [2, 2048, 2048], P(None, 'dp', 'tp'), may hold values from -0.125 to 0.125
- lam_re: float32 [2, 128, 64], P(None, 'tp'), may hold values from -1 to -0.05
- lam_im: float32 [2, 128, 64], P(None, 'tp'), may hold values from 0 to 6
- log_dt: float32 [2, 128], P(None, 'tp'), may hold values from -3 to 0
- b_re: float32 [2, 128, 64, 16], P(None, 'tp'), may hold values from -1 to 1
- b_im: float32 [2, 128, 64, 16], P(None, 'tp'), may hold values from -1 to 1
- readout_real: float32 [2, 128, 16, 64], P(None, 'tp'), may hold values from -0.5 to 0.5
- readout_imaginary: float32 [2, 128, 16, 64], P(None, 'tp'), may hold values from -0.5 to 0.5
- d_skip: float32 [2, 2048], P(None, 'tp'), may hold values from -4 to 4
- w_val: bfloat16 [2, 2048, 2048], P(None, 'tp', 'dp'), may hold values from -0.375 to 0.375
- w_gate: bfloat16 [2, 2048, 2048], P(None, 'tp', 'dp'), may hold values from -0.375 to 0.375
- state: float32 [2, 256, 128, 128], P(None, 'dp', 'tp'), may hold values from -6 to 6
Outputs:
- stream_out: bfloat16 [256, 2048], P('tp', 'dp')
- states_out: float32 [2, 256, 128, 128], P(None, 'dp', 'tp')
All inputs are finite; a program needn't handle non-finite values.
Results may differ from a plain program's by a relative error of at most 0.0064.
Values may be sent and summed in bfloat16 or wider, within the bound.
A program may use at most 64 MiB of HBM per device.

v0:
```python
import jax
import jax.numpy as jnp
from jax import lax
from jax.sharding import PartitionSpec as P

D = 2048
LAYERS = 2
eps = 1e-06


def advance(
    inputs, old_state, lam_re, lam_im, log_dt, b_re, b_im, readout_real, readout_imaginary, d_skip
):
    upper_bound = lax.Precision.HIGHEST
    count_rows, groups, doubled = old_state.shape
    half_state = doubled // 2
    chans = b_re.shape[-1]
    step_size = jnp.exp(log_dt)[:, None]
    decay = jnp.exp(lam_re * step_size)
    angle = lam_im * step_size
    keep_re = decay * jnp.cos(angle)
    keep_im = decay * jnp.sin(angle)
    denom = lam_re * lam_re + lam_im * lam_im
    ratio_re = ((keep_re - 1.0) * lam_re + keep_im * lam_im) / denom
    ratio_im = (keep_im * lam_re - (keep_re - 1.0) * lam_im) / denom
    drive_re = ratio_re[..., None] * b_re - ratio_im[..., None] * b_im
    drive_im = ratio_re[..., None] * b_im + ratio_im[..., None] * b_re
    grouped = inputs.reshape(count_rows, groups, chans)
    push_re = jnp.einsum("gpc,rgc->rgp", drive_re, grouped, precision=upper_bound)
    push_im = jnp.einsum("gpc,rgc->rgp", drive_im, grouped, precision=upper_bound)
    old_re = old_state[..., :half_state]
    old_im = old_state[..., half_state:]
    updated_real = keep_re * old_re - keep_im * old_im + push_re
    updated_imaginary = keep_re * old_im + keep_im * old_re + push_im
    readout_output = jnp.einsum(
        "aot,mat->mao", readout_real, updated_real, precision=upper_bound
    ) - jnp.einsum("aot,mat->mao", readout_imaginary, updated_imaginary, precision=upper_bound)
    pre_act = readout_output.reshape(count_rows, groups * chans) + d_skip * inputs
    return (pre_act, jnp.concatenate([updated_real, updated_imaginary], axis=-1))


def half_output(mixed_all, val_part, gate_part):
    return jnp.concatenate(
        [
            jnp.dot(mixed_all, val_part, preferred_element_type=jnp.float32),
            jnp.dot(mixed_all, gate_part, preferred_element_type=jnp.float32),
        ],
        axis=1,
    )


def per_device(
    stream,
    norm_gain,
    w_input,
    lam_re,
    lam_im,
    log_dt,
    b_re,
    b_im,
    readout_real,
    readout_imaginary,
    d_skip,
    w_val,
    w_gate,
    state,
):
    collected = []
    for layer_no in range(LAYERS):
        gathered = lax.all_gather(stream, "tp", axis=0, tiled=True)
        widened = gathered.astype(jnp.float32)
        normed = (widened * norm_gain[layer_no]).astype(jnp.bfloat16)
        square_part = jnp.sum(widened * widened, axis=1)
        weight_in = w_input[layer_no]
        partial_value = jnp.dot(normed, weight_in, preferred_element_type=jnp.float32)
        summed, square_total = (
            lax.psum_scatter(partial_value, "dp", scatter_dimension=0, tiled=True),
            lax.psum_scatter(square_part, "dp", scatter_dimension=0, tiled=True),
        )
        inputs = lax.rsqrt(square_total / D + eps)[:, None] * summed
        pre_act, new_state = advance(
            inputs,
            state[layer_no],
            lam_re[layer_no],
            lam_im[layer_no],
            log_dt[layer_no],
            b_re[layer_no],
            b_im[layer_no],
            readout_real[layer_no],
            readout_imaginary[layer_no],
            d_skip[layer_no],
        )
        mixed = jax.nn.gelu(pre_act).astype(jnp.bfloat16)
        mixed_all = lax.all_gather(mixed, "dp", axis=0, tiled=True)
        columns = w_val.shape[2]
        combined = lax.psum_scatter(
            half_output(mixed_all, w_val[layer_no], w_gate[layer_no]),
            "tp",
            scatter_dimension=0,
            tiled=True,
        )
        value = combined[:, :columns]
        gate = combined[:, columns:]
        stream = (stream.astype(jnp.float32) + value * jax.nn.sigmoid(gate)).astype(jnp.bfloat16)
        collected.append(new_state)
    return (stream, jnp.stack(collected))


def solution(mesh):
    return jax.shard_map(
        per_device,
        mesh=mesh,
        in_specs=(
            P("tp", "dp"),
            P(None, "dp"),
            P(None, "dp", "tp"),
            P(None, "tp", None),
            P(None, "tp", None),
            P(None, "tp"),
            P(None, "tp", None, None),
            P(None, "tp", None, None),
            P(None, "tp", None, None),
            P(None, "tp", None, None),
            P(None, "tp"),
            P(None, "tp", "dp"),
            P(None, "tp", "dp"),
            P(None, "dp", "tp", None),
        ),
        out_specs=(P("tp", "dp"), P(None, "dp", "tp", None)),
        check_vma=False,
    )
```

profile of v0, /device:TPU:0, one launch (start us, length us, event | category | flops | bytes accessed | tf_op | source)
XLA Modules:
  0.0 278.8 jit_solution(17151186009216203104)
XLA Ops:
  7.2 0.0 reduce-scatter.5.cloned.1.call-start
  7.2 0.8 fusion.109
  8.0 32.8 %all_gather.12 = bf16[256,512]{1,0:T(8,128)(2,1)S(1)} all-gather(bf16[32,512]{1,0:T(8,128)(2,1)} %param.14), channel_id=1, replica_groups=mesh['tp'=8,'dp'=4] {'tp'}, dimensions={0}, use_global_device_ids=true | all-gather | bytes 294912 | tf_op jit(solution)/shard_map/all_gather | solution.py:70
  40.8 1.9 fusion.10
  42.7 0.0 reduce-scatter.5.cloned.1.call-update
  42.7 0.0 reduce-scatter.7.cloned.1.call-start
  42.8 0.7 copy-done.18
  43.4 0.1 multiply_bitcast_fusion.1
  43.6 0.2 fusion.93
  43.8 0.1 fusion.4
  43.9 0.5 copy-done.17
  44.4 5.6 %all-reduce = f32[256]{0:T(256)S(1)} all-reduce(f32[256]{0:T(256)S(1)} %fusion.4), channel_id=2, replica_groups=mesh['tp'=8,'dp'=4] {'dp'}, use_global_device_ids=true, to_apply=%region_1.0.clone | all-reduce | flops 256 | bytes 2048
  50.1 0.7 copy-done.19
  50.7 0.6 dynamic-slice
  52.0 0.1 fusion.106
  52.0 0.1 fusion.108
  52.1 0.3 copy_bitcast_fusion
  52.5 11.4 %reduce-scatter.5.cloned.1.call-done = f32[64,256]{1,0:T(8,128)} async-done(((f32[256,256]{1,0:T(8,128)}), f32[64,256]{1,0:T(8,128)}) %reduce-scatter.5.cloned.1.call-update) | async-done | bytes 65552 | tf_op jit(solution)/shard_map/reduce_scatter | solution.py:77
  63.9 0.9 broadcast_multiply_fusion.1
  64.8 0.1 copy.33
  64.9 1.0 fusion.3
  65.9 1.0 fusion.2
  67.0 0.9 fusion.38
  67.9 0.0 copy-done.8
  68.0 0.9 convolution_subtract_fusion.1
  68.9 0.1 copy.34
  69.0 0.8 copy-done.10
  69.7 0.1 fusion.63
  69.8 5.5 %all_gather.13 = bf16[256,256]{1,0:T(8,128)(2,1)S(1)} all-gather(bf16[64,256]{1,0:T(8,128)(2,1)S(1)} %fusion.63), channel_id=1, replica_groups=mesh['tp'=8,'dp'=4] {'dp'}, dimensions={0}, use_global_device_ids=true | all-gather | bytes 163840 | tf_op jit(solution)/shard_map/all_gather | solution.py:94
  75.4 0.2 fusion.17
  75.6 0.2 fusion.19
  75.9 1.1 pad_maximum_fusion
  76.9 0.0 reduce-scatter.7.cloned.1.call-update
  77.0 0.0 reduce-scatter.9.cloned.1.call-start
  77.0 64.3 %reduce-scatter.7.cloned.1.call-done = f32[32,1024]{1,0:T(8,128)} async-done(((f32[256,1024]{1,0:T(8,128)}), f32[32,1024]{1,0:T(8,128)}) %reduce-scatter.7.cloned.1.call-update) | async-done | bytes 131088 | tf_op jit(solution)/shard_map/reduce_scatter | solution.py:96
  141.4 0.9 fusion.90
  142.3 30.9 %all_gather.14 = bf16[256,512]{1,0:T(8,128)(2,1)S(1)} all-gather(bf16[32,512]{1,0:T(8,128)(2,1)S(1)} %fusion.90), channel_id=1, replica_groups=mesh['tp'=8,'dp'=4] {'tp'}, dimensions={0}, use_global_device_ids=true | all-gather | bytes 294912 | tf_op jit(solution)/shard_map/all_gather | solution.py:70
  173.1 0.9 fusion.8
  174.1 0.0 reduce-scatter.11.cloned.1.call-start
  174.1 0.1 fusion.6
  174.3 5.7 %all-reduce.1 = f32[256]{0:T(256)S(1)} all-reduce(f32[256]{0:T(256)S(1)} %fusion.6), channel_id=5, replica_groups=mesh['tp'=8,'dp'=4] {'dp'}, use_global_device_ids=true, to_apply=%region_5.0.clone | all-reduce | flops 256 | bytes 2048
  179.9 0.1 fusion.107
  180.0 13.2 %reduce-scatter.9.cloned.1.call-done = f32[64,256]{1,0:T(8,128)} async-done(((f32[256,256]{1,0:T(8,128)}), f32[64,256]{1,0:T(8,128)}) %reduce-scatter.9.cloned.1.call-update) | async-done | bytes 65552 | tf_op jit(solution)/shard_map/reduce_scatter | solution.py:77
  193.2 0.9 broadcast_multiply_fusion
  194.2 0.1 copy.36
  194.3 1.0 fusion
  195.3 1.0 fusion.1
  196.4 0.9 fusion.31
  197.3 0.0 copy-done.9
  197.3 0.9 convolution_subtract_fusion
  198.3 0.1 copy.37
  198.4 0.8 copy-done.11
  199.1 0.1 fusion.71
  199.2 5.5 %all_gather.15 = bf16[256,256]{1,0:T(8,128)(2,1)S(1)} all-gather(bf16[64,256]{1,0:T(8,128)(2,1)S(1)} %fusion.71), channel_id=1, replica_groups=mesh['tp'=8,'dp'=4] {'dp'}, dimensions={0}, use_global_device_ids=true | all-gather | bytes 163840 | tf_op jit(solution)/shard_map/all_gather | solution.py:94
  204.8 0.2 fusion.12
  205.0 0.2 fusion.14
  205.2 1.1 pad_maximum_fusion.1
  206.3 0.0 reduce-scatter.11.cloned.1.call-update
  206.3 0.2 maximum_bitcast_fusion
  206.5 0.2 maximum_bitcast_fusion.1
  206.8 0.1 pad_maximum_fusion.2
  206.9 1.6 copy.38
  208.5 62.3 %reduce-scatter.11.cloned.1.call-done = f32[32,1024]{1,0:T(8,128)} async-done(((f32[256,1024]{1,0:T(8,128)}), f32[32,1024]{1,0:T(8,128)}) %reduce-scatter.11.cloned.1.call-update) | async-done | bytes 131088 | tf_op jit(solution)/shard_map/reduce_scatter | solution.py:96
  270.7 1.5 fusion.91
  (36 shorter events, 0.1 us)
Async XLA Ops:
  7.2 44.9 %copy-start.2 = (f32[2,64,16,128]{3,2,1,0:T(8,128)S(1)}, f32[2,64,16,128]{3,2,1,0:T(8,128)}, u32[]{:S(2)}) copy-start(f32[2,64,16,128]{3,2,1,0:T(8,128)} %param.27) | copy-start | bytes 3145732
  7.2 56.7 %reduce-scatter.5.cloned.1.call-start = ((), (), s32[]{:S(2)}) async-start(), calls=%async_computation.4 | async-start | bytes 327680 | tf_op jit(solution)/shard_map/reduce_scatter | solution.py:77
  42.7 0.8 copy-start.15
  42.7 0.8 copy-start.16
  42.7 98.7 %reduce-scatter.7.cloned.1.call-start = ((), (), s32[]{:S(2)}) async-start(), calls=%async_computation.5 | async-start | bytes 1179648 | tf_op jit(solution)/shard_map/reduce_scatter | solution.py:96
  42.7 0.7 copy-start.18
  43.7 0.7 copy-start.17
  50.1 0.7 copy-start.19
  52.1 12.7 %copy-start.1 = (f32[2,16,64,16]{2,3,1,0:T(8,128)S(1)}, f32[2,16,64,16]{2,3,1,0:T(8,128)}, u32[]{:S(2)}) copy-start(f32[2,16,64,16]{2,3,1,0:T(8,128)} %param.20) | copy-start | bytes 393220
  52.5 12.4 %copy-start = (f32[2,16,64,16]{2,3,1,0:T(8,128)S(1)}, f32[2,16,64,16]{2,3,1,0:T(8,128)}, u32[]{:S(2)}) copy-start(f32[2,16,64,16]{2,3,1,0:T(8,128)} %param.21) | copy-start | bytes 393220
  65.9 1.1 copy-start.12
  67.0 1.0 copy-start.8
  68.0 7.5 %copy-start.4 = (bf16[2,256,512]{2,1,0:T(8,128)(2,1)S(1)}, bf16[2,256,512]{2,1,0:T(8,128)(2,1)}, u32[]{:S(2)}) copy-start(bf16[2,256,512]{2,1,0:T(8,128)(2,1)} %param.26) | copy-start | bytes 1572868
  68.9 0.9 copy-start.10
  69.8 5.8 %copy-start.6 = (bf16[2,256,512]{2,1,0:T(8,128)(2,1)S(1)}, bf16[2,256,512]{2,1,0:T(8,128)(2,1)}, u32[]{:S(2)}) copy-start(bf16[2,256,512]{2,1,0:T(8,128)(2,1)} %param.25) | copy-start | bytes 1572868
  76.9 64.4 %copy-start.14 = (bf16[32,512]{1,0:T(8,128)(2,1)S(1)}, bf16[32,512]{1,0:T(8,128)(2,1)}, u32[]{:S(2)}) copy-start(bf16[32,512]{1,0:T(8,128)(2,1)} %param.14) | copy-start | bytes 98308
  76.9 96.2 %copy-start.3 = (bf16[2,512,256]{2,1,0:T(8,128)(2,1)S(1)}, bf16[2,512,256]{2,1,0:T(8,128)(2,1)}, u32[]{:S(2)}) copy-start(bf16[2,512,256]{2,1,0:T(8,128)(2,1)} %param.16) | copy-start | bytes 1572868
  77.0 116.3 %reduce-scatter.9.cloned.1.call-start = ((), (), s32[]{:S(2)}) async-start(), calls=%async_computation.6 | async-start | bytes 327680 | tf_op jit(solution)/shard_map/reduce_scatter | solution.py:77
  174.1 96.6 %reduce-scatter.11.cloned.1.call-start = ((), (), s32[]{:S(2)}) async-start(), calls=%async_computation.7 | async-start | bytes 1179648 | tf_op jit(solution)/shard_map/reduce_scatter | solution.py:96
  195.3 1.1 copy-start.13
  196.4 1.0 copy-start.9
  197.3 7.4 %copy-start.5 = (bf16[2,256,512]{2,1,0:T(8,128)(2,1)S(1)}, bf16[2,256,512]{2,1,0:T(8,128)(2,1)}, u32[]{:S(2)}) copy-start(bf16[2,256,512]{2,1,0:T(8,128)(2,1)} %param.26) | copy-start | bytes 1572868
  198.3 0.9 copy-start.11
  199.2 5.8 %copy-start.7 = (bf16[2,256,512]{2,1,0:T(8,128)(2,1)S(1)}, bf16[2,256,512]{2,1,0:T(8,128)(2,1)}, u32[]{:S(2)}) copy-start(bf16[2,256,512]{2,1,0:T(8,128)(2,1)} %param.25) | copy-start | bytes 1572868
Sparse Core Ops, SparseCore 0:
  42.8 21.0 reduce-scatter.4
  77.1 64.2 reduce-scatter.6
  174.2 18.9 reduce-scatter.8
  206.5 64.2 reduce-scatter.10
where the time goes:
time: 279 us
  waiting for transfers between devices  151 us (54%)
  blocking collectives  86 us (31%)
  between operations  14.7 us (5%)
  matrix products  11.6 us (4%)
  other arithmetic  7.83 us (3%)
  local copies, waits for them, and re-layouts  7.2 us (3%)
    reduce_scatter x2, waiting for transfers between devices, per_device(): lax.psum_scatter(half_output(mixed_all, w_val[layer_no], w_gate[layer_no]...  127 us
    all_gather x2, blocking collectives, per_device(): gathered = lax.all_gather(stream, 'tp', axis=0, tiled=True)  63.6 us
    reduce_scatter x2, waiting for transfers between devices, per_device(): lax.psum_scatter(partial_value, 'dp', scatter_dimension=0, tiled=True)  24.6 us
    unnamed x2, blocking collectives  11.3 us
    all_gather x2, blocking collectives, per_device(): mixed_all = lax.all_gather(mixed, 'dp', axis=0, tiled=True)  11.1 us
    unnamed x42, local copies, waits for them, and re-layouts  5.66 us
  transfers between devices with their start and end apart: 4, of which 4 were waited for; matrix products, arithmetic and copies ran while one was open for 1% of the time, Pallas kernels for 0%

commit v1 on v0

--- a/solution.py
+++ b/solution.py
@@ -6,6 +6,29 @@
 D = 2048
 LAYERS = 2
 eps = 1e-06
+
+
+def define_words(u, along_dim):
+    u = jnp.moveaxis(u, 0, along_dim)
+    y = u.shape
+    return u.reshape(*y[:along_dim], y[along_dim] * y[along_dim + 1], *y[along_dim + 2 :])
+
+
+def table_balance(m, comm_axis):
+    latest = jax.lax.axis_size(comm_axis)
+    inter, arr_now = (latest, jax.lax.axis_index(comm_axis))
+    val2, outer = (m[None], 1)
+    while outer < inter:
+        series = []
+        for k0 in range(inter):
+            series.append((k0, k0 ^ outer))
+        outcome_arr = jax.lax.ppermute(val2, axis_name=comm_axis, perm=series)
+        y1 = arr_now & outer == 0
+        step_out = jnp.where(y1, val2, outcome_arr)
+        block_last = jnp.where(y1, outcome_arr, val2)
+        val2 = jnp.concatenate([step_out, block_last])
+        outer *= 2
+    return val2
 
 
 def advance(
@@ -67,7 +90,8 @@
 ):
     collected = []
     for layer_no in range(LAYERS):
-        gathered = lax.all_gather(stream, "tp", axis=0, tiled=True)
+        y_new = table_balance(stream, "tp")
+        gathered = define_words(y_new, 0)
         widened = gathered.astype(jnp.float32)
         normed = (widened * norm_gain[layer_no]).astype(jnp.bfloat16)
         square_part = jnp.sum(widened * widened, axis=1)

time: 279 us -> 249 us (0.89)
  blocking collectives: 86 us -> 22.4 us
  waiting for transfers between devices: 151 us -> 173 us
  starting transfers between devices: 0.16 us -> 11.8 us
    all_gather x2 -> x0, blocking collectives: 63.6 us -> none  [per_device(): gathered = lax.all_gather(stream, 'tp', axis=0, tiled=True)]
    ppermute x0 -> x6, waiting for transfers between devices: none -> 19.1 us  [table_balance(): outcome_arr = jax.lax.ppermute(val2, axis_name=comm_axis, perm=series)]
    ppermute x0 -> x6, starting transfers between devices: none -> 11.6 us  [table_balance(): outcome_arr = jax.lax.ppermute(val2, axis_name=comm_axis, perm=series)]
    reduce_scatter x2, waiting for transfers between devices: 24.6 us -> 27.5 us  [per_device(): lax.psum_scatter(partial_value, 'dp', scatter_dimension=0, tiled=True)]
    unnamed x42 -> x44, local copies, waits for them, and re-layouts: 5.66 us -> 5.05 us
  transfers between devices with their start and end apart: 4 -> 10, of which waited for: 4 -> 10; matrix products, arithmetic and copies ran while one was open for 1% -> 2% of each run, Pallas kernels for 0% -> 0%
where the time goes in v1:
time: 249 us; the launch traced here: 248 us
  waiting for transfers between devices  173 us (69%)
  blocking collectives  22.4 us (9%)
  between operations  14.8 us (6%)
  starting transfers between devices  11.8 us (5%)
  matrix products  10.6 us (4%)
  other arithmetic  7.98 us (3%)
  local copies, waits for them, and re-layouts  7.18 us (3%)
    reduce_scatter x2, waiting for transfers between devices, per_device(): lax.psum_scatter(half_output(mixed_all, w_val[layer_no], w_gate[layer_no]...  127 us
    reduce_scatter x2, waiting for transfers between devices, per_device(): lax.psum_scatter(partial_value, 'dp', scatter_dimension=0, tiled=True)  27.5 us
    ppermute x6, waiting for transfers between devices, table_balance(): outcome_arr = jax.lax.ppermute(val2, axis_name=comm_axis, perm=series)  19.1 us
    ppermute x6, starting transfers between devices, table_balance(): outcome_arr = jax.lax.ppermute(val2, axis_name=comm_axis, perm=series)  11.6 us
    unnamed x2, blocking collectives  11.3 us
    all_gather x2, blocking collectives, per_device(): mixed_all = lax.all_gather(mixed, 'dp', axis=0, tiled=True)  11.1 us
    unnamed x44, local copies, waits for them, and re-layouts  5.05 us
  transfers between devices with their start and end apart: 10, of which 10 were waited for; matrix products, arithmetic and copies ran while one was open for 2% of the time, Pallas kernels for 0%

profile of v1, /device:TPU:0, one launch (start us, length us, event | category | flops | bytes accessed | tf_op | source)
XLA Modules:
  0.0 248.1 jit_solution(7049027057876351220)
XLA Ops:
  7.2 3.1 %collective-permute-start = (bf16[1,32,512]{2,1,0:T(8,128)(2,1)}, bf16[1,32,512]{2,1,0:T(8,128)(2,1)S(1)}, u32[]{:S(2)}, u32[]{:S(2)}) collective-permute-start(bf16[1,32,512]{2,1,0:T(8,128)(2,1)} %bitcast.262), channel_id=1, source_target_pairs={{0,4},{4,0},{8,12},{12,8},{16,20},{20,16},{24,28},{28,24},{1,5},{5... | collective-permute-start | bytes 98312 | tf_op jit(solution)/shard_map/ppermute | solution.py:25
  10.3 1.3 fusion.104
  11.6 0.1 multiply_bitcast_fusion.1
  11.8 0.6 collective-permute-done
  12.4 2.1 collective-permute-start.1
  14.6 0.2 fusion.89
  14.7 0.6 copy-done.20
  15.4 0.6 dynamic-slice
  16.6 0.2 collective-permute-done.1
  16.9 3.1 %collective-permute-start.2 = (bf16[4,32,512]{2,1,0:T(8,128)(2,1)S(1)}, bf16[4,32,512]{2,1,0:T(8,128)(2,1)S(1)}, u32[]{:S(2)}, u32[]{:S(2)}) collective-permute-start(bf16[4,32,512]{2,1,0:T(8,128)(2,1)S(1)} %pad_maximum_fusion.5), channel_id=1, source_target_pairs={{0,16},{4,20},{8,24},{12,28},{16,0},{20,4},{24,8},{28,12},{1,17},{... | collective-permute-start | bytes 393224 | tf_op jit(solution)/shard_map/ppermute | solution.py:25
  20.0 4.7 %collective-permute-done.2 = bf16[4,32,512]{2,1,0:T(8,128)(2,1)S(1)} collective-permute-done((bf16[4,32,512]{2,1,0:T(8,128)(2,1)S(1)}, bf16[4,32,512]{2,1,0:T(8,128)(2,1)S(1)}, u32[]{:S(2)}, u32[]{:S(2)}) %collective-permute-start.2) | collective-permute-done | bytes 131104 | tf_op jit(solution)/shard_map/ppermute | solution.py:25
  24.7 0.1 fusion.4
  24.8 0.9 fusion.18
  25.8 0.6 copy-done.18
  26.4 0.3 copy_bitcast_fusion
  26.8 0.1 reduce_sum.23
  26.9 5.6 %all-reduce = f32[256]{0:T(256)S(1)} all-reduce(f32[256]{0:T(256)S(1)} %reduce_sum.23), channel_id=2, replica_groups=mesh['tp'=8,'dp'=4] {'dp'}, use_global_device_ids=true, to_apply=%region_1.2.clone | all-reduce | flops 256 | bytes 2048
  32.5 0.1 fusion.102
  32.6 14.6 %reduce-scatter.5.cloned.1.call-done = f32[64,256]{1,0:T(8,128)} async-done(((f32[256,256]{1,0:T(8,128)}), f32[64,256]{1,0:T(8,128)}) %reduce-scatter.5.cloned.1.call-update) | async-done | bytes 65552 | tf_op jit(solution)/shard_map/reduce_scatter | solution.py:101
  47.1 0.9 broadcast_multiply_fusion.1
  48.0 0.1 copy.33
  48.2 1.0 fusion.3
  49.2 1.0 fusion.2
  50.3 0.9 fusion.34
  51.2 0.9 convolution_subtract_fusion.1
  52.2 0.1 copy.34
  52.2 0.8 copy-done.10
  53.0 0.1 fusion.59
  53.1 5.5 %all_gather.6 = bf16[256,256]{1,0:T(8,128)(2,1)S(1)} all-gather(bf16[64,256]{1,0:T(8,128)(2,1)S(1)} %fusion.59), channel_id=1, replica_groups=mesh['tp'=8,'dp'=4] {'dp'}, dimensions={0}, use_global_device_ids=true | all-gather | bytes 163840 | tf_op jit(solution)/shard_map/all_gather | solution.py:118
  58.7 0.2 fusion.14
  58.9 0.2 fusion.16
  59.1 1.1 pad_maximum_fusion
  60.3 64.3 %reduce-scatter.7.cloned.1.call-done = f32[32,1024]{1,0:T(8,128)} async-done(((f32[256,1024]{1,0:T(8,128)}), f32[32,1024]{1,0:T(8,128)}) %reduce-scatter.7.cloned.1.call-update) | async-done | bytes 131088 | tf_op jit(solution)/shard_map/reduce_scatter | solution.py:120
  124.6 0.9 fusion.86
  125.5 1.2 collective-permute-start.3
  126.7 2.8 %collective-permute-done.3 = bf16[1,32,512]{2,1,0:T(8,128)(2,1)S(1)} collective-permute-done((bf16[1,32,512]{2,1,0:T(8,128)(2,1)S(1)}, bf16[1,32,512]{2,1,0:T(8,128)(2,1)S(1)}, u32[]{:S(2)}, u32[]{:S(2)}) %collective-permute-start.3) | collective-permute-done | bytes 32800 | tf_op jit(solution)/shard_map/ppermute | solution.py:25
  129.5 1.4 collective-permute-start.4
  130.9 4.3 %collective-permute-done.4 = bf16[2,32,512]{2,1,0:T(8,128)(2,1)S(1)} collective-permute-done((bf16[2,32,512]{2,1,0:T(8,128)(2,1)S(1)}, bf16[2,32,512]{2,1,0:T(8,128)(2,1)S(1)}, u32[]{:S(2)}, u32[]{:S(2)}) %collective-permute-start.4) | collective-permute-done | bytes 65568 | tf_op jit(solution)/shard_map/ppermute | solution.py:25
  135.3 0.8 collective-permute-start.5
  136.1 6.5 %collective-permute-done.5 = bf16[4,32,512]{2,1,0:T(8,128)(2,1)S(1)} collective-permute-done((bf16[4,32,512]{2,1,0:T(8,128)(2,1)S(1)}, bf16[4,32,512]{2,1,0:T(8,128)(2,1)S(1)}, u32[]{:S(2)}, u32[]{:S(2)}) %collective-permute-start.5) | collective-permute-done | bytes 131104 | tf_op jit(solution)/shard_map/ppermute | solution.py:25
  142.6 0.1 fusion.6
  142.8 0.9 fusion.12
  143.8 0.1 reduce_sum.25
  143.9 5.6 %all-reduce.1 = f32[256]{0:T(256)S(1)} all-reduce(f32[256]{0:T(256)S(1)} %reduce_sum.25), channel_id=5, replica_groups=mesh['tp'=8,'dp'=4] {'dp'}, use_global_device_ids=true, to_apply=%region_5.6.clone | all-reduce | flops 256 | bytes 2048
  149.5 0.1 fusion.103
  149.6 13.0 %reduce-scatter.9.cloned.1.call-done = f32[64,256]{1,0:T(8,128)} async-done(((f32[256,256]{1,0:T(8,128)}), f32[64,256]{1,0:T(8,128)}) %reduce-scatter.9.cloned.1.call-update) | async-done | bytes 65552 | tf_op jit(solution)/shard_map/reduce_scatter | solution.py:101
  162.6 0.9 broadcast_multiply_fusion
  163.5 0.1 copy.36
  163.6 1.0 fusion
  164.6 1.0 fusion.1
  165.7 0.9 fusion.27
  166.6 0.9 convolution_subtract_fusion
  167.6 0.1 copy.37
  167.7 0.8 copy-done.11
  168.4 0.1 fusion.67
  168.5 5.5 %all_gather.7 = bf16[256,256]{1,0:T(8,128)(2,1)S(1)} all-gather(bf16[64,256]{1,0:T(8,128)(2,1)S(1)} %fusion.67), channel_id=1, replica_groups=mesh['tp'=8,'dp'=4] {'dp'}, dimensions={0}, use_global_device_ids=true | all-gather | bytes 163840 | tf_op jit(solution)/shard_map/all_gather | solution.py:118
  174.1 0.2 fusion.8
  174.3 0.2 fusion.10
  174.6 1.1 pad_maximum_fusion.1
  175.7 0.2 maximum_bitcast_fusion
  175.9 0.2 maximum_bitcast_fusion.1
  176.2 1.6 copy.38
  177.7 62.3 %reduce-scatter.11.cloned.1.call-done = f32[32,1024]{1,0:T(8,128)} async-done(((f32[256,1024]{1,0:T(8,128)}), f32[32,1024]{1,0:T(8,128)}) %reduce-scatter.11.cloned.1.call-update) | async-done | bytes 131088 | tf_op jit(solution)/shard_map/reduce_scatter | solution.py:120
  240.0 1.5 fusion.87
  (60 shorter events, 0.6 us)
Async XLA Ops:
  7.2 3.1 %copy-start.19 = (f32[2,16]{1,0:T(2,128)S(1)}, f32[2,16]{1,0:T(2,128)}, u32[]{:S(2)}) copy-start(f32[2,16]{1,0:T(2,128)} %param.19) | copy-start | bytes 388
  7.2 40.0 %reduce-scatter.5.cloned.1.call-start = ((), (), s32[]{:S(2)}) async-start(), calls=%async_computation.4 | async-start | bytes 327680 | tf_op jit(solution)/shard_map/reduce_scatter | solution.py:101
  7.2 5.2 %collective-permute-start = (bf16[1,32,512]{2,1,0:T(8,128)(2,1)}, bf16[1,32,512]{2,1,0:T(8,128)(2,1)S(1)}, u32[]{:S(2)}, u32[]{:S(2)}) collective-permute-start(bf16[1,32,512]{2,1,0:T(8,128)(2,1)} %bitcast.262), channel_id=1, source_target_pairs={{0,4},{4,0},{8,12},{12,8},{16,20},{20,16},{24,28},{28,24},{1,5},{5... | collective-permute-start | bytes 98312 | tf_op jit(solution)/shard_map/ppermute | solution.py:25
  10.3 1.3 copy-start.15
  10.3 1.3 copy-start.16
  11.6 0.8 copy-start.14
  12.4 4.4 %collective-permute-start.1 = (bf16[2,32,512]{2,1,0:T(8,128)(2,1)S(1)}, bf16[2,32,512]{2,1,0:T(8,128)(2,1)S(1)}, u32[]{:S(2)}, u32[]{:S(2)}) collective-permute-start(bf16[2,32,512]{2,1,0:T(8,128)(2,1)S(1)} %pad_maximum_fusion.7), channel_id=1, source_target_pairs={{0,8},{4,12},{8,0},{12,4},{16,24},{20,28},{24,16},{28,20},{1,9},{5... | collective-permute-start | bytes 196616 | tf_op jit(solution)/shard_map/ppermute | solution.py:25
  14.7 0.7 copy-start.20
  16.8 3.1 %copy-start.17 = (f32[2,512]{1,0:T(2,128)S(1)}, f32[2,512]{1,0:T(2,128)}, u32[]{:S(2)}) copy-start(f32[2,512]{1,0:T(2,128)} %param.15) | copy-start | bytes 12292
  16.9 7.8 %collective-permute-start.2 = (bf16[4,32,512]{2,1,0:T(8,128)(2,1)S(1)}, bf16[4,32,512]{2,1,0:T(8,128)(2,1)S(1)}, u32[]{:S(2)}, u32[]{:S(2)}) collective-permute-start(bf16[4,32,512]{2,1,0:T(8,128)(2,1)S(1)} %pad_maximum_fusion.5), channel_id=1, source_target_pairs={{0,16},{4,20},{8,24},{12,28},{16,0},{20,4},{24,8},{28,12},{1,17},{... | collective-permute-start | bytes 393224 | tf_op jit(solution)/shard_map/ppermute | solution.py:25
  20.0 4.8 %copy-start.2 = (bf16[2,512,256]{2,1,0:T(8,128)(2,1)S(1)}, bf16[2,512,256]{2,1,0:T(8,128)(2,1)}, u32[]{:S(2)}) copy-start(bf16[2,512,256]{2,1,0:T(8,128)(2,1)} %param.16) | copy-start | bytes 1572868
  25.8 0.7 copy-start.18
  25.8 98.8 %reduce-scatter.7.cloned.1.call-start = ((), (), s32[]{:S(2)}) async-start(), calls=%async_computation.5 | async-start | bytes 1179648 | tf_op jit(solution)/shard_map/reduce_scatter | solution.py:120
  26.4 21.7 %copy-start.1 = (f32[2,16,64,16]{2,3,1,0:T(8,128)S(1)}, f32[2,16,64,16]{2,3,1,0:T(8,128)}, u32[]{:S(2)}) copy-start(f32[2,16,64,16]{2,3,1,0:T(8,128)} %param.20) | copy-start | bytes 393220
  26.8 21.4 %copy-start = (f32[2,16,64,16]{2,3,1,0:T(8,128)S(1)}, f32[2,16,64,16]{2,3,1,0:T(8,128)}, u32[]{:S(2)}) copy-start(f32[2,16,64,16]{2,3,1,0:T(8,128)} %param.21) | copy-start | bytes 393220
  49.2 1.1 copy-start.12
  50.3 1.0 copy-start.8
  51.2 7.5 %copy-start.4 = (bf16[2,256,512]{2,1,0:T(8,128)(2,1)S(1)}, bf16[2,256,512]{2,1,0:T(8,128)(2,1)}, u32[]{:S(2)}) copy-start(bf16[2,256,512]{2,1,0:T(8,128)(2,1)} %param.26) | copy-start | bytes 1572868
  52.1 0.9 copy-start.10
  53.1 5.8 %copy-start.6 = (bf16[2,256,512]{2,1,0:T(8,128)(2,1)S(1)}, bf16[2,256,512]{2,1,0:T(8,128)(2,1)}, u32[]{:S(2)}) copy-start(bf16[2,256,512]{2,1,0:T(8,128)(2,1)} %param.25) | copy-start | bytes 1572868
  60.2 102.3 %reduce-scatter.9.cloned.1.call-start = ((), (), s32[]{:S(2)}) async-start(), calls=%async_computation.6 | async-start | bytes 327680 | tf_op jit(solution)/shard_map/reduce_scatter | solution.py:101
  125.5 4.0 %collective-permute-start.3 = (bf16[1,32,512]{2,1,0:T(8,128)(2,1)S(1)}, bf16[1,32,512]{2,1,0:T(8,128)(2,1)S(1)}, u32[]{:S(2)}, u32[]{:S(2)}) collective-permute-start(bf16[1,32,512]{2,1,0:T(8,128)(2,1)S(1)} %bitcast.261), channel_id=1, source_target_pairs={{0,4},{4,0},{8,12},{12,8},{16,20},{20,16},{24,28},{28,24},{1,5},{5... | collective-permute-start | bytes 98312 | tf_op jit(solution)/shard_map/ppermute | solution.py:25
  129.5 5.7 %collective-permute-start.4 = (bf16[2,32,512]{2,1,0:T(8,128)(2,1)S(1)}, bf16[2,32,512]{2,1,0:T(8,128)(2,1)S(1)}, u32[]{:S(2)}, u32[]{:S(2)}) collective-permute-start(bf16[2,32,512]{2,1,0:T(8,128)(2,1)S(1)} %pad_maximum_fusion.8), channel_id=1, source_target_pairs={{0,8},{4,12},{8,0},{12,4},{16,24},{20,28},{24,16},{28,20},{1,9},{5... | collective-permute-start | bytes 196616 | tf_op jit(solution)/shard_map/ppermute | solution.py:25
  135.2 7.5 %copy-start.3 = (bf16[2,512,256]{2,1,0:T(8,128)(2,1)S(1)}, bf16[2,512,256]{2,1,0:T(8,128)(2,1)}, u32[]{:S(2)}) copy-start(bf16[2,512,256]{2,1,0:T(8,128)(2,1)} %param.16) | copy-start | bytes 1572868
  135.3 7.3 %collective-permute-start.5 = (bf16[4,32,512]{2,1,0:T(8,128)(2,1)S(1)}, bf16[4,32,512]{2,1,0:T(8,128)(2,1)S(1)}, u32[]{:S(2)}, u32[]{:S(2)}) collective-permute-start(bf16[4,32,512]{2,1,0:T(8,128)(2,1)S(1)} %pad_maximum_fusion.6), channel_id=1, source_target_pairs={{0,16},{4,20},{8,24},{12,28},{16,0},{20,4},{24,8},{28,12},{1,17},{... | collective-permute-start | bytes 393224 | tf_op jit(solution)/shard_map/ppermute | solution.py:25
  143.7 96.3 %reduce-scatter.11.cloned.1.call-start = ((), (), s32[]{:S(2)}) async-start(), calls=%async_computation.7 | async-start | bytes 1179648 | tf_op jit(solution)/shard_map/reduce_scatter | solution.py:120
  164.6 1.1 copy-start.13
  165.7 1.0 copy-start.9
  166.6 7.4 %copy-start.5 = (bf16[2,256,512]{2,1,0:T(8,128)(2,1)S(1)}, bf16[2,256,512]{2,1,0:T(8,128)(2,1)}, u32[]{:S(2)}) copy-start(bf16[2,256,512]{2,1,0:T(8,128)(2,1)} %param.26) | copy-start | bytes 1572868
  167.6 0.9 copy-start.11
  168.5 5.8 %copy-start.7 = (bf16[2,256,512]{2,1,0:T(8,128)(2,1)S(1)}, bf16[2,256,512]{2,1,0:T(8,128)(2,1)}, u32[]{:S(2)}) copy-start(bf16[2,256,512]{2,1,0:T(8,128)(2,1)} %param.25) | copy-start | bytes 1572868
Sparse Core Ops, SparseCore 0:
  25.9 21.1 reduce-scatter.4
  60.3 64.2 reduce-scatter.6
  143.9 18.6 reduce-scatter.8
  175.8 64.1 reduce-scatter.10
